TPU v7x, 32 devices: a whole 2x2x4 slice. The times are simulated.
32 devices in a mesh: ep: 32 (over z, y, x, core).
Axes of the slice: x: 2, y: 2, z: 4, core: 2. Of those that a mesh axis runs over, the one named last changes fastest.
Arguments:
- tokens: bfloat16 [640, 2048], P('ep'), may hold values from -6 to 6
- positions: int32 [640], P('ep'), may hold values from 1024 to 16383
- state: float32 [640, 8, 64, 128], P('ep'), may hold values from -1.6 to 1.6
- mix_gain: float32 [2048], replicated, may hold values from 0.1 to 1.9
- w_query: bfloat16 [2048, 512], replicated, may hold values from -0.125 to 0.125
- w_key: bfloat16 [2048, 512], replicated, may hold values from -0.125 to 0.125
- w_value: bfloat16 [2048, 1024], replicated, may hold values from -0.125 to 0.125
- ret_gain: float32 [1024], replicated, may hold values from 0.1 to 1.9
- w_out: bfloat16 [1024, 2048], P(None, 'ep'), may hold values from -0.1875 to 0.1875
- ffn_gain: float32 [2048], replicated, may hold values from 0.1 to 1.9
- routes: int32 [640, 6], P('ep'), may hold values from 0 to 31, all different within a row; in each aligned block of 20 rows (0 to 19, 20 to 39, ...) at most 7 rows name the same one
- route_weights: float32 [640, 6], P('ep'), may hold values from 0.1 to 1
- expert_gate: bfloat16 [32, 2048, 512], P('ep'), may hold values from -0.125 to 0.125
- expert_up: bfloat16 [32, 2048, 512], P('ep'), may hold values from -0.125 to 0.125
- expert_down: bfloat16 [32, 512, 2048], P('ep'), may hold values from -0.25 to 0.25
Outputs:
- result: bfloat16 [640, 2048], P('ep')
- new_state: float32 [640, 8, 64, 128], P('ep')
Inputs may be any that keep to these rules, and one draw needn't show every extreme that they name: `routes`: each row names 6 different experts; among the rows of one device no expert is named more than 7 times, a bound that some block reaches there.
All inputs are finite; a program needn't handle non-finite values.
Results may differ from a plain program's by a relative error of at most 0.017.
Values may be sent and summed in bfloat16 or wider, within the bound.
A program may use at most 128 MiB of HBM per device.

v0:
```python
import math

import jax
import jax.numpy as jnp
from jax import lax
from jax.sharding import PartitionSpec as P

EPS = 1e-06


def rms_scale(values, gain):
    wide = values.astype(jnp.float32)
    scaled = wide * lax.rsqrt(jnp.mean(wide * wide, axis=-1, keepdims=True) + EPS)
    return (scaled * gain).astype(jnp.bfloat16)


def rotate(field, spots):
    half = field.shape[-1] // 2
    freqs = jnp.exp(-math.log(10000.0) * jnp.arange(half, dtype=jnp.float32) / half)
    angle = spots.astype(jnp.float32)[:, None] * freqs[None, :]
    cosine = jnp.cos(angle)[:, None, :]
    sine = jnp.sin(angle)[:, None, :]
    first = field[..., :half]
    second = field[..., half:]
    return jnp.concatenate(
        [first * cosine - second * sine, second * cosine + first * sine], axis=-1
    )


def shards(
    tokens,
    positions,
    state,
    mix_gain,
    w_query,
    w_key,
    w_value,
    ret_gain,
    w_out,
    ffn_gain,
    routes,
    route_weights,
    expert_gate,
    expert_up,
    expert_down,
):
    seqs = tokens.shape[0]
    width = tokens.shape[1]
    heads = state.shape[1]
    head_k = state.shape[2]
    head_v = state.shape[3]
    normed_in = rms_scale(tokens, mix_gain)
    q_proj = jnp.dot(normed_in, w_query, preferred_element_type=jnp.float32).astype(jnp.bfloat16)
    k_proj = jnp.dot(normed_in, w_key, preferred_element_type=jnp.float32).astype(jnp.bfloat16)
    v_proj = jnp.dot(normed_in, w_value, preferred_element_type=jnp.float32).astype(jnp.bfloat16)
    queries = rotate(q_proj.astype(jnp.float32).reshape(seqs, heads, head_k), positions)
    key_rows = rotate(
        k_proj.astype(jnp.float32).reshape(seqs, heads, head_k), positions
    ) * head_k ** (-0.5)
    values = v_proj.astype(jnp.float32).reshape(seqs, heads, head_v)
    decays = 1.0 - jnp.exp2(-2.0 - jnp.arange(heads, dtype=jnp.float32))
    new_state = (
        decays[None, :, None, None] * state + key_rows[:, :, :, None] * values[:, :, None, :]
    )
    readout = jnp.einsum("thd,thdv->thv", queries, new_state, precision=lax.Precision.HIGHEST)
    centre = jnp.mean(readout, axis=-1, keepdims=True)
    variance = jnp.mean(jnp.square(readout - centre), axis=-1, keepdims=True)
    normed = ((readout - centre) * lax.rsqrt(variance + EPS)).reshape(
        seqs, heads * head_v
    ) * ret_gain
    mixed = normed.astype(jnp.bfloat16)
    attended = jnp.dot(
        mixed, lax.all_gather(w_out, "ep", axis=1, tiled=True), preferred_element_type=jnp.float32
    ).astype(jnp.bfloat16)
    resid = (tokens.astype(jnp.float32) + attended.astype(jnp.float32)).astype(jnp.bfloat16)
    normed_mid = rms_scale(resid, ffn_gain)
    topk = routes.shape[1]
    row_count = seqs * topk
    held = expert_gate.shape[0]
    experts = held * lax.axis_size("ep")
    capacity = max(2, 2 * row_count // experts)
    chosen = routes.reshape(row_count)
    matches = (chosen[:, None] == jnp.arange(experts, dtype=jnp.int32)[None, :]).astype(jnp.int32)
    places = jnp.sum((jnp.cumsum(matches, axis=0) - matches) * matches, axis=1)
    slots = chosen * capacity + places
    dispatch = (slots[:, None] == jnp.arange(experts * capacity, dtype=jnp.int32)[None, :]).astype(
        jnp.bfloat16
    )
    repeated = jnp.repeat(normed_mid, topk, axis=0)
    outgoing = jnp.einsum("rs,rd->sd", dispatch, repeated, preferred_element_type=jnp.float32)
    outgoing = outgoing.astype(jnp.bfloat16).reshape(experts, capacity, width)
    arrivals = lax.all_to_all(outgoing, "ep", split_axis=0, concat_axis=0, tiled=True)
    senders = arrivals.shape[0] // held
    grouped = arrivals.reshape(senders, held, arrivals.shape[1], width)
    gate_part = jnp.einsum(
        "necd,edf->necf", grouped, expert_gate, preferred_element_type=jnp.float32
    )
    up_part = jnp.einsum("necd,edf->necf", grouped, expert_up, preferred_element_type=jnp.float32)
    hidden = (jax.nn.silu(gate_part) * up_part).astype(jnp.bfloat16)
    down_part = jnp.einsum(
        "necf,efd->necd", hidden, expert_down, preferred_element_type=jnp.float32
    )
    served = down_part.astype(jnp.bfloat16).reshape(arrivals.shape)
    returned = lax.all_to_all(served, "ep", split_axis=0, concat_axis=0, tiled=True)
    picked_rows = jnp.dot(
        dispatch, returned.reshape(experts * capacity, width), preferred_element_type=jnp.float32
    )
    mixture = jnp.sum(picked_rows.reshape(seqs, topk, width) * route_weights[:, :, None], axis=1)
    result = (resid.astype(jnp.float32) + mixture).astype(jnp.bfloat16)
    return (result, new_state)


def solution(mesh):
    placed = (
        P("ep", None),
        P("ep"),
        P("ep", None, None, None),
        P(),
        P(),
        P(),
        P(),
        P(),
        P(None, "ep"),
        P(),
        P("ep", None),
        P("ep", None),
        P("ep", None, None),
        P("ep", None, None),
        P("ep", None, None),
    )
    return jax.shard_map(
        shards,
        mesh=mesh,
        in_specs=placed,
        out_specs=(P("ep", None), P("ep", None, None, None)),
        check_vma=False,
    )
```

profile of v0, /device:TPU:0, one launch (start us, length us, event | category | flops | bytes accessed | tf_op | source)
XLA Modules:
  0.0 159.3 jit_solution(1809398466089321715)
XLA Ops:
  7.2 0.7 all-gather.2.cloned.1.call-update
  7.9 1.0 fusion.39
  9.0 2.1 %fusion.27 = f32[20,512]{1,0:T(8,128)S(1)} fusion(bf16[2048,512]{1,0:T(8,128)(2,1)} %param.19, bf16[20,2048]{1,0:T(8,128)(2,1)} %param.15, f32[2048]{0:T(1024)} %param.18, f32[20]{0:T(128)S(1)} %add_rsqrt_fusion.2), kind=kOutput, calls=%fused_computation.25 | convolution fusion | flops 42127360 | bytes 2228304 | tf_op jit(solution)/shard_map/dot_general | solution.py:53
  11.2 2.0 %fusion.26 = f32[20,512]{1,0:T(8,128)S(1)} fusion(bf16[2048,512]{1,0:T(8,128)(2,1)} %param.20, bf16[20,2048]{1,0:T(8,128)(2,1)S(1)} %copy-done.3, f32[2048]{0:T(1024)S(1)} %copy-done.5, f32[20]{0:T(128)S(1)} %add_rsqrt_fusion.2), kind=kOutput, calls=%fused_computation.23 | convolution fusion | flops 42127360 | bytes 2228304 | tf_op jit(solution)/shard_map/dot_general | solution.py:54
  13.3 3.0 %fusion.25 = f32[20,1024]{1,0:T(8,128)S(1)} fusion(bf16[2048,1024]{1,0:T(8,128)(2,1)} %param.21, bf16[20,2048]{1,0:T(8,128)(2,1)S(1)} %copy-done.3, f32[2048]{0:T(1024)S(1)} %copy-done.5, f32[20]{0:T(128)S(1)} %add_rsqrt_fusion.2), kind=kOutput, calls=%fused_computation.21 | convolution fusion | flops 84090880 | bytes 4366416 | tf_op jit(solution)/shard_map/dot_general | solution.py:55
  16.9 0.2 copy-done.2
  17.1 1.7 %multiply_add_fusion = f32[20,8,64,128]{3,2,1,0:T(8,128)S(1)} fusion(f32[20,8,64,128]{3,2,1,0:T(8,128)S(1)} %copy-done.2, f32[20,8,128]{2,1,0:T(8,128)S(1)} %slice.20, f32[20,8,64]{2,1,0:T(8,128)S(1)} %maximum_multiply_fusion, f32[8]{0:T(128)S(1)} %exponential_subtract_fusion), kind=kLoop, calls=%fused_computation | loop fusion | flops 3932160 | bytes 10608672 | tf_op jit(solution)/shard_map/add | solution.py:63
  18.8 4.6 %fusion.52 = f32[20,8,1,128]{3,2,1,0:T(1,128)S(1)} fusion(f32[20,8,64,1]{2,3,1,0:T(1,128)S(1)} %bitcast.77, f32[20,8,64,128]{3,2,1,0:T(8,128)S(1)} %multiply_add_fusion), kind=kOutput, calls=%fused_computation.71 | convolution fusion | flops 15728640 | bytes 5365760 | tf_op jit(solution)/shard_map/thd,thdv->thv/dot_general | solution.py:65
  24.3 0.2 select_reduce_fusion
  24.5 50.9 %all-gather.2.cloned.1.call-done = bf16[1024,2048]{0,1:T(8,128)(2,1)} async-done(((bf16[1024,64]{0,1:T(8,128)(2,1)}), bf16[1024,2048]{0,1:T(8,128)(2,1)}) %all-gather.2.cloned.1.call-update) | async-done | bytes 4194320 | tf_op jit(solution)/shard_map/all_gather | solution.py:73
  75.4 3.5 %multiply_reduce_fusion = (f32[20]{0:T(128)S(1)}, f32[20,2048]{1,0:T(8,128)S(1)}) fusion(bf16[1024,2048]{0,1:T(8,128)(2,1)} %all-gather.2.cloned.1.call-done, f32[20,1024]{1,0:T(8,128)S(1)} %bitcast.74, f32[1024]{0:T(1024)S(1)} %copy-done.8, bf16[20,2048]{1,0:T(8,128)(2,1)S(1)} %copy-done.3), kind=kOutput, calls=%fused_computation.41 | convolution fusion | flops 84254704 | bytes 4526160 | tf_op jit(solution)/shard_map/dot_general | solution.py:72
  79.1 0.2 reshape.195
  79.2 1.4 convolution_convert_fusion.1
  80.7 1.5 reshape.196
  82.2 29.4 %all_to_all.10 = bf16[32,7,2048]{2,1,0:T(8,128)(2,1)S(1)} all-to-all(bf16[32,7,2048]{2,1,0:T(8,128)(2,1)S(1)} %reshape.196), channel_id=1, replica_groups=mesh['ep'=32] {'ep'}, dimensions={0} | all-to-all | bytes 1835008 | tf_op jit(solution)/shard_map/all_to_all | solution.py:92
  111.6 1.0 copy-done.4
  112.6 1.7 %fusion.10 = f32[32,1,7,512]{3,0,2,1:T(8,128)} fusion(bf16[1,2048,512]{2,1,0:T(8,128)(2,1)S(1)} %copy-done.9, bf16[32,7,2048]{2,1,0:T(8,128)(2,1)S(1)} %all_to_all.10), kind=kOutput, calls=%fused_computation.15 | convolution fusion | flops 469762048 | bytes 3473408 | tf_op jit(solution)/shard_map/necd,edf->necf/dot_general | solution.py:95
  114.2 3.4 %convolution_convert_fusion = bf16[32,7,2048]{2,0,1:T(8,128)(2,1)S(1)} fusion(bf16[1,512,2048]{2,1,0:T(8,128)(2,1)S(1)} %copy-done, bf16[1,2048,512]{2,1,0:T(8,128)(2,1)} %param.28, bf16[32,7,2048]{2,1,0:T(8,128)(2,1)} %copy-done.4, f32[32,1,7,512]{3,0,2,1:T(8,128)} %fusion.10), kind=kOutput, calls=%fused_computation.1 | convolution fusion | flops 940670976 | bytes 6488064 | tf_op jit(solution)/shard_map/necf,efd->necd/dot_general | solution.py:100
  117.7 1.5 copy.42
  119.2 3.6 %all-to-all-start.1 = ((bf16[32,7,2048]{2,1,0:T(8,128)(2,1)}), bf16[32,7,2048]{2,1,0:T(8,128)(2,1)S(1)}, u32[]{:S(2)}, u32[]{:S(2)}) async-start(bf16[32,7,2048]{2,1,0:T(8,128)(2,1)} %copy.42), calls=%async_computation.1 | async-start | bytes 2097152 | tf_op jit(solution)/shard_map/all_to_all | solution.py:104
  123.0 26.0 %all-to-all-done.1 = bf16[32,7,2048]{2,1,0:T(8,128)(2,1)S(1)} async-done(((bf16[32,7,2048]{2,1,0:T(8,128)(2,1)}), bf16[32,7,2048]{2,1,0:T(8,128)(2,1)S(1)}, u32[]{:S(2)}, u32[]{:S(2)}) %all-to-all-start.1) | async-done | bytes 917536 | tf_op jit(solution)/shard_map/all_to_all | solution.py:104
  149.0 1.2 reshape.212
  150.3 1.6 fusion.9
  151.8 0.7 add_convert_fusion
  (53 shorter events, 2.0 us)
Async XLA Ops:
  7.2 107.1 %copy-start = (bf16[1,512,2048]{2,1,0:T(8,128)(2,1)S(1)}, bf16[1,512,2048]{2,1,0:T(8,128)(2,1)}, u32[]{:S(2)}) copy-start(bf16[1,512,2048]{2,1,0:T(8,128)(2,1)} %param.29) | copy-start | bytes 6291460
  7.2 4.0 %copy-start.3 = (bf16[20,2048]{1,0:T(8,128)(2,1)S(1)}, bf16[20,2048]{1,0:T(8,128)(2,1)}, u32[]{:S(2)}) copy-start(bf16[20,2048]{1,0:T(8,128)(2,1)} %param.15) | copy-start | bytes 245764
  7.2 4.0 %copy-start.5 = (f32[2048]{0:T(1024)S(1)}, f32[2048]{0:T(1024)}, u32[]{:S(2)}) copy-start(f32[2048]{0:T(1024)} %param.18) | copy-start | bytes 24580
  7.2 68.1 %all-gather.2.cloned.1.call-start = ((), (), s32[]{:S(2)}) async-start(), calls=%async_computation.2 | async-start | bytes 4325376 | tf_op jit(solution)/shard_map/all_gather | solution.py:73
  9.0 4.3 %copy-start.11 = (s32[20]{0:T(128)S(1)}, s32[20]{0:T(128)}, u32[]{:S(2)}) copy-start(s32[20]{0:T(128)} %param.16) | copy-start | bytes 244
  13.3 3.8 %copy-start.2 = (f32[20,8,64,128]{3,2,1,0:T(8,128)S(1)}, f32[20,8,64,128]{3,2,1,0:T(8,128)}, u32[]{:S(2)}) copy-start(f32[20,8,64,128]{3,2,1,0:T(8,128)} %param.17) | copy-start | bytes 15728644
  18.7 4.6 %copy-start.1 = (f32[20,8,64,128]{3,2,1,0:T(8,128)}, f32[20,8,64,128]{3,2,1,0:T(8,128)S(1)}, u32[]{:S(2)}) copy-start(f32[20,8,64,128]{3,2,1,0:T(8,128)S(1)} %multiply_add_fusion) | copy-start | bytes 15728644
  18.8 5.1 %copy-start.6 = (s32[20,6]{0,1:T(8,128)S(1)}, s32[20,6]{0,1:T(8,128)}, u32[]{:S(2)}) copy-start(s32[20,6]{0,1:T(8,128)} %param.25) | copy-start | bytes 1444
  18.8 56.6 %copy-start.8 = (f32[1024]{0:T(1024)S(1)}, f32[1024]{0:T(1024)}, u32[]{:S(2)}) copy-start(f32[1024]{0:T(1024)} %param.22) | copy-start | bytes 12292
  75.3 3.5 %copy-start.7 = (f32[2048]{0:T(1024)S(1)}, f32[2048]{0:T(1024)}, u32[]{:S(2)}) copy-start(f32[2048]{0:T(1024)} %param.24) | copy-start | bytes 24580
  82.2 30.4 %copy-start.9 = (bf16[1,2048,512]{2,1,0:T(8,128)(2,1)S(1)}, bf16[1,2048,512]{2,1,0:T(8,128)(2,1)}, u32[]{:S(2)}) copy-start(bf16[1,2048,512]{2,1,0:T(8,128)(2,1)} %param.27) | copy-start | bytes 6291460
  111.6 1.0 copy-start.4
  119.2 31.1 %copy-start.10 = (f32[20,6]{0,1:T(8,128)S(1)}, f32[20,6]{0,1:T(8,128)}, u32[]{:S(2)}) copy-start(f32[20,6]{0,1:T(8,128)} %param.26) | copy-start | bytes 1444
  119.2 29.8 %all-to-all-start.1 = ((bf16[32,7,2048]{2,1,0:T(8,128)(2,1)}), bf16[32,7,2048]{2,1,0:T(8,128)(2,1)S(1)}, u32[]{:S(2)}, u32[]{:S(2)}) async-start(bf16[32,7,2048]{2,1,0:T(8,128)(2,1)} %copy.42), calls=%async_computation.1 | async-start | bytes 2097152 | tf_op jit(solution)/shard_map/all_to_all | solution.py:104
Sparse Core Ops, SparseCore 0:
  10.9 64.4 all-gather.1
where the time goes:
time: 160 us; the launch traced here: 159 us
  waiting for transfers between devices  77.6 us (48%)
  blocking collectives  29.4 us (18%)
  matrix products  23.4 us (15%)
  between operations  14.3 us (9%)
  local copies, waits for them, and re-layouts  6.26 us (4%)
  other arithmetic  4.73 us (3%)
  starting transfers between devices  3.66 us (2%)
    all_gather x1, waiting for transfers between devices, shards(): lax.all_gather(w_out, 'ep', axis=1, tiled=True)  50.9 us
    all_to_all x1, blocking collectives, shards(): lax.all_to_all(outgoing, 'ep', split_axis=0, concat_axis=0, tiled=True)  29.4 us
    all_to_all x1, waiting for transfers between devices, shards(): lax.all_to_all(served, 'ep', split_axis=0, concat_axis=0, tiled=True)  26 us
    dot_general x1, matrix products, shards(): jnp.einsum('thd,thdv->thv', queries, new_state, precision=lax.Precision.H...  4.59 us
    all_to_all x1, starting transfers between devices, shards(): lax.all_to_all(served, 'ep', split_axis=0, concat_axis=0, tiled=True)  3.63 us
    dot_general x1, matrix products, shards(): jnp.dot(mixed, lax.all_gather(w_out, 'ep', axis=1, tiled=True), preferred...  3.51 us
    dot_general x1, matrix products, shards(): jnp.einsum('necf,efd->necd', hidden, expert_down, preferred_element_type=...  3.42 us
  transfers between devices with their start and end apart: 2, of which 2 were waited for; matrix products, arithmetic and copies ran while one was open for 10% of the time, Pallas kernels for 0%

commit v1 on v0

v1 whole, which is shorter than its diff:
```python
import functools
import math

import jax
import jax.numpy as jnp
from jax import lax
from jax.experimental import pallas as pl
from jax.experimental.pallas import tpu as pltpu
from jax.sharding import PartitionSpec as P

EPS = 1e-06
MESH = pl.DeviceIdType.MESH
PAD = 8
VMEM_LIMIT = 64 * 1024 * 1024 - 128 * 1024


def layout_of(mesh):
    devices = list(mesh.devices.flat)
    count = len(devices)
    try:
        far = [max(d.coords[i] for d in devices) - min(d.coords[i] for d in devices) + 1 for i in range(3)]
        cores = count // (far[0] * far[1] * far[2])
        if cores * far[0] * far[1] * far[2] == count and cores >= 1:
            return (far[2], far[1], far[0], cores)
    except (AttributeError, TypeError, IndexError):
        pass
    cores = 2 if count % 2 == 0 else 1
    chips = count // cores
    side = 1
    while (side * 2) ** 2 * 4 <= chips and chips % ((side * 2) ** 2) == 0:
        side *= 2
    return (chips // (side * side), side, side, cores)


class Place:
    def __init__(self, dims):
        self.dims = dims
        depth, rows, cols, cores = dims
        me = lax.axis_index("ep")
        self.me = me
        self.spot = (
            me // (rows * cols * cores),
            (me // (cols * cores)) % rows,
            (me // cores) % cols,
            me % cores,
        )

    def at(self, dz, dy, dx, dc=0):
        total = 0
        for size, here, move in zip(self.dims, self.spot, (dz, dy, dx, dc)):
            total = total * size + (here + move) % size if move % size else total * size + here
        return total

    def greet(self):
        depth, rows, cols, cores = self.dims
        moves = [(d, 0, 0, 0) for d in range(1, depth)]
        moves += [(0, d, 0, 0) for d in range(1, rows)]
        moves += [(0, 0, d, 0) for d in range(1, cols)]
        moves += [(0, 0, 0, d) for d in range(1, cores)]
        barrier = pltpu.get_barrier_semaphore()
        for move in moves:
            pl.semaphore_signal(barrier, inc=1, device_id=(self.at(*move),), device_id_type=MESH)
        pl.semaphore_wait(barrier, len(moves))


def gather_names(dims):
    depth, rows, cols, cores = dims
    names = []
    for dz in range(depth):
        if dz:
            names.append(("z", dz, 0, 0, 0))
        for dx in range(1, cols):
            names.append(("x", dz, 0, dx, 0))
        for dy in range(1, rows):
            names.append(("y", dz, dy, 0, 0))
            for dx in range(1, cols):
                names.append(("p", dz, dy, dx, 0))
                names.append(("q", dz, dy, dx, 0))
        for dy in range(rows):
            for dx in range(cols):
                for dc in range(1, cores):
                    names.append(("c", dz, dy, dx, dc))
    return {name: i for i, name in enumerate(names)}


class Gather:
    def __init__(self, place, view, send, recv):
        self.place, self.view, self.send, self.recv = place, view, send, recv
        self.names = gather_names(place.dims)
        self.sent = []

    def copy(self, name):
        kind, dz, dy, dx, dc = name
        m = self.names[name]
        back = {"z": (-dz, 0, 0, 0), "x": (0, 0, -dx, 0), "y": (0, -dy, 0, 0)}
        back.update({"p": (0, -dy, 0, 0), "q": (0, 0, -dx, 0), "c": (0, 0, 0, -dc)})
        return m, {"p": 0, "q": 1}.get(kind), self.place.at(*back[kind])

    def put(self, name, held):
        m, half, target = self.copy(name)
        ref = self.view(self.place.at(*held), half)
        c = pltpu.make_async_remote_copy(
            src_ref=ref, dst_ref=ref, send_sem=self.send.at[m], recv_sem=self.recv.at[m],
            device_id=(target,), device_id_type=MESH,
        )
        c.start()
        self.sent.append(c)

    def get(self, name):
        m, half, target = self.copy(name)
        ref = self.view(self.place.at(*name[1:]), half)
        pltpu.make_async_remote_copy(
            src_ref=ref, dst_ref=ref, send_sem=self.send.at[m], recv_sem=self.recv.at[m],
            device_id=(target,), device_id_type=MESH,
        ).wait_recv()

    def mates(self, dz, dy, dx):
        for dc in range(1, self.place.dims[3]):
            self.put(("c", dz, dy, dx, dc), (dz, dy, dx, 0))

    def first(self, dz):
        depth, rows, cols, cores = self.place.dims
        if dz == 0:
            for d in range(1, depth):
                self.put(("z", d, 0, 0, 0), (0, 0, 0, 0))
        else:
            self.get(("z", dz, 0, 0, 0))
        for dx in range(1, cols):
            self.put(("x", dz, 0, dx, 0), (dz, 0, 0, 0))
        for dy in range(1, rows):
            self.put(("y", dz, dy, 0, 0), (dz, 0, 0, 0))
        self.mates(dz, 0, 0)

    def second(self, dz):
        depth, rows, cols, cores = self.place.dims
        for dx in range(1, cols):
            self.get(("x", dz, 0, dx, 0))
            for dy in range(1, rows):
                self.put(("p", dz, dy, dx, 0), (dz, 0, dx, 0))
            self.mates(dz, 0, dx)
        for dy in range(1, rows):
            self.get(("y", dz, dy, 0, 0))
            for dx in range(1, cols):
                self.put(("q", dz, dy, dx, 0), (dz, dy, 0, 0))
            self.mates(dz, dy, 0)

    def third(self, dz):
        depth, rows, cols, cores = self.place.dims
        for dy in range(1, rows):
            for dx in range(1, cols):
                self.get(("p", dz, dy, dx, 0))
                self.get(("q", dz, dy, dx, 0))
                self.mates(dz, dy, dx)

    def fourth(self, dz):
        depth, rows, cols, cores = self.place.dims
        for dy in range(rows):
            for dx in range(cols):
                for dc in range(1, cores):
                    self.get(("c", dz, dy, dx, dc))

    def finish(self):
        for c in self.sent:
            c.wait_send()


def halves(ref, width):
    cut = -(-width // 256) * 128
    spans = {None: (0, width), 0: (0, cut), 1: (cut, width - cut)}

    def view(index, half):
        start, size = spans[half]
        return ref.at[index, :, pl.ds(start, size)]

    return view


def gather_kernel(dims, own, out, load, send, recv):
    place = Place(dims)
    fill = pltpu.make_async_copy(own, out.at[place.me], load)
    fill.start()
    place.greet()
    fill.wait()
    g = Gather(place, halves(out, out.shape[2]), send, recv)
    depth = dims[0]
    for t in range(depth + 3):
        if t < depth:
            g.first(t)
        if 0 <= t - 1 < depth:
            g.second(t - 1)
        if 0 <= t - 2 < depth:
            g.third(t - 2)
        if 0 <= t - 3 < depth:
            g.fourth(t - 3)
    g.finish()


def gather_blocks(dims, block, collective):
    count = math.prod(dims)
    messages = len(gather_names(dims))
    return pl.pallas_call(
        functools.partial(gather_kernel, dims),
        out_shape=jax.ShapeDtypeStruct((count,) + block.shape, block.dtype),
        in_specs=[pl.BlockSpec(memory_space=pl.ANY)],
        out_specs=pl.BlockSpec(memory_space=pltpu.VMEM),
        scratch_shapes=[
            pltpu.SemaphoreType.DMA,
            pltpu.SemaphoreType.DMA((messages,)),
            pltpu.SemaphoreType.DMA((messages,)),
        ],
        compiler_params=pltpu.CompilerParams(
            collective_id=collective, has_side_effects=True, vmem_limit_bytes=VMEM_LIMIT
        ),
        name="gather_blocks",
    )(block)


class Reduce:
    def __init__(self, place, parts, slots, send, recv):
        self.place, self.parts, self.slots, self.send, self.recv = place, parts, slots, send, recv
        self.names = gather_names(place.dims)
        self.sent = []
        self.width = parts.shape[2]

    def span(self, half):
        cut = self.width // 2
        return {None: pl.ds(0, self.width), 0: pl.ds(0, cut), 1: pl.ds(cut, self.width - cut)}[half]

    def copy(self, name):
        kind, dz, dy, dx, dc = name
        m = self.names[name]
        ahead = {"z": (dz, 0, 0, 0), "x": (0, 0, dx, 0), "y": (0, dy, 0, 0)}
        ahead.update({"p": (0, dy, 0, 0), "q": (0, 0, dx, 0), "c": (0, 0, 0, dc)})
        cols = self.span({"p": 0, "q": 1}.get(kind))
        return pltpu.make_async_remote_copy(
            src_ref=self.parts.at[self.place.at(dz, dy, dx, dc), :, cols],
            dst_ref=self.slots.at[m, :, cols],
            send_sem=self.send.at[m], recv_sem=self.recv.at[m],
            device_id=(self.place.at(*ahead[kind]),), device_id_type=MESH,
        )

    def put(self, name):
        c = self.copy(name)
        c.start()
        self.sent.append(c)

    def get(self, name):
        kind = name[0]
        self.copy(name).wait_recv()
        cols = self.span({"p": 0, "q": 1}.get(kind))
        return self.slots[self.names[name], :, cols].astype(jnp.float32)

    def add(self, index, cols, terms):
        value = self.parts[index, :, cols].astype(jnp.float32)
        for term in terms:
            value = value + term
        self.parts[index, :, cols] = value.astype(self.parts.dtype)

    def zeroth(self, dz):
        depth, rows, cols, cores = self.place.dims
        order = sorted(((dy, dx) for dy in range(rows) for dx in range(cols)), key=lambda o: (not o[0]) + (not o[1]))
        for dy, dx in order:
            for dc in range(1, cores):
                self.put(("c", dz, dy, dx, dc))

    def first(self, dz):
        depth, rows, cols, cores = self.place.dims
        order = sorted(((dy, dx) for dy in range(rows) for dx in range(cols)), key=lambda o: (not o[0]) + (not o[1]))
        for dy, dx in order:
            terms = [self.get(("c", dz, dy, dx, dc)) for dc in range(1, cores)]
            if terms:
                self.add(self.place.at(dz, dy, dx), self.span(None), terms)
            if dy and dx:
                self.put(("p", dz, dy, dx, 0))
                self.put(("q", dz, dy, dx, 0))

    def second(self, dz):
        depth, rows, cols, cores = self.place.dims
        for dx in range(1, cols):
            terms = [self.get(("p", dz, dy, dx, 0)) for dy in range(1, rows)]
            if terms:
                self.add(self.place.at(dz, 0, dx), self.span(0), terms)
            self.put(("x", dz, 0, dx, 0))
        for dy in range(1, rows):
            terms = [self.get(("q", dz, dy, dx, 0)) for dx in range(1, cols)]
            if terms:
                self.add(self.place.at(dz, dy, 0), self.span(1), terms)
            self.put(("y", dz, dy, 0, 0))

    def third(self, dz):
        depth, rows, cols, cores = self.place.dims
        terms = [self.get(("x", dz, 0, dx, 0)) for dx in range(1, cols)]
        terms += [self.get(("y", dz, dy, 0, 0)) for dy in range(1, rows)]
        if dz:
            if terms:
                self.add(self.place.at(dz, 0, 0), self.span(None), terms)
            self.put(("z", dz, 0, 0, 0))
            return None
        value = self.parts[self.place.me].astype(jnp.float32)
        for term in terms:
            value = value + term
        return value

    def finish(self):
        for c in self.sent:
            c.wait_send()


def experts_kernel(
    dims, seqs, width, own, resid, gate_hbm, up_hbm, down_hbm, out,
    held, parts, slots, gate, up, down, mine, load, send, recv, back_send, back_recv,
):
    place = Place(dims)
    depth, rows, cols, cores = dims
    count = math.prod(dims)
    plane = rows * cols * cores
    fills = [
        pltpu.make_async_copy(a, b, load.at[i])
        for i, (a, b) in enumerate(
            [(own, held.at[place.me]), (gate_hbm.at[0], gate), (up_hbm.at[0], up), (down_hbm.at[0], down), (resid, mine)]
        )
    ]
    for fill in fills:
        fill.start()
    place.greet()
    fills[0].wait()
    g = Gather(place, halves(held, held.shape[2]), send, recv)
    r = Reduce(place, parts, slots, back_send, back_recv)
    padded = held.shape[1]
    step = max(1, 192 // padded)
    while plane % step:
        step -= 1

    def serve(dz):
        base = ((place.spot[0] + dz) % depth) * plane
        extra = held.shape[2] - width
        lane = lax.broadcasted_iota(jnp.int32, (step * padded, extra), 1)
        pick = jnp.logical_or(lane == place.me, lane == place.me + count)
        for k in range(0, plane, step):
            some = held[pl.ds(base + k, step)].reshape(step * padded, held.shape[2])
            rows_in = some[:, :width]
            scale = jnp.sum(
                jnp.where(pick, some[:, width:].astype(jnp.float32), 0.0), axis=1, keepdims=True
            )
            gate_part = jnp.dot(rows_in, gate[...], preferred_element_type=jnp.float32)
            up_part = jnp.dot(rows_in, up[...], preferred_element_type=jnp.float32)
            hidden = (gate_part * jax.nn.sigmoid(gate_part) * up_part).astype(jnp.bfloat16)
            served = jnp.dot(hidden, down[...], preferred_element_type=jnp.float32) * scale
            parts[pl.ds(base + k, step)] = served.astype(jnp.bfloat16).reshape(step, padded, width)

    total = None
    for t in range(depth + 6):
        if t < depth:
            g.first(t)
        if 0 <= t - 1 < depth:
            g.second(t - 1)
        if 0 <= t - 2 < depth:
            g.third(t - 2)
        if 0 <= t - 3 < depth:
            g.fourth(t - 3)
            if t == 3:
                for fill in fills[1:]:
                    fill.wait()
            serve(t - 3)
            r.zeroth(t - 3)
        if 0 <= t - 4 < depth:
            r.first(t - 4)
        if 0 <= t - 5 < depth:
            r.second(t - 5)
        if 0 <= t - 6 < depth:
            value = r.third(t - 6)
            total = value if value is not None else total
    for dz in range(1, depth):
        total = total + r.get(("z", dz, 0, 0, 0))
    out[...] = (mine[...].astype(jnp.float32) + total[:seqs]).astype(out.dtype)
    g.finish()
    r.finish()


def experts(dims, block, resid, gate, up, down, collective):
    count = math.prod(dims)
    seqs, width = resid.shape
    messages = len(gather_names(dims))
    padded = block.shape[0]
    anywhere = pl.BlockSpec(memory_space=pl.ANY)
    return pl.pallas_call(
        functools.partial(experts_kernel, dims, seqs, width),
        out_shape=jax.ShapeDtypeStruct(resid.shape, resid.dtype),
        in_specs=[anywhere] * 5,
        out_specs=pl.BlockSpec(memory_space=pltpu.VMEM),
        scratch_shapes=[
            pltpu.VMEM((count,) + block.shape, block.dtype),
            pltpu.VMEM((count, padded, width), jnp.bfloat16),
            pltpu.VMEM((messages, padded, width), jnp.bfloat16),
            pltpu.VMEM(gate.shape[1:], gate.dtype),
            pltpu.VMEM(up.shape[1:], up.dtype),
            pltpu.VMEM(down.shape[1:], down.dtype),
            pltpu.VMEM(resid.shape, resid.dtype),
            pltpu.SemaphoreType.DMA((5,)),
        ] + [pltpu.SemaphoreType.DMA((messages,))] * 4,
        compiler_params=pltpu.CompilerParams(
            collective_id=collective, has_side_effects=True, vmem_limit_bytes=VMEM_LIMIT
        ),
        name="experts",
    )(block, resid, gate, up, down)


def rms_scale(values, gain):
    wide = values.astype(jnp.float32)
    scaled = wide * lax.rsqrt(jnp.mean(wide * wide, axis=-1, keepdims=True) + EPS)
    return (scaled * gain).astype(jnp.bfloat16)


def rotate(field, spots):
    half = field.shape[-1] // 2
    freqs = jnp.exp(-math.log(10000.0) * jnp.arange(half, dtype=jnp.float32) / half)
    angle = spots.astype(jnp.float32)[:, None] * freqs[None, :]
    cosine = jnp.cos(angle)[:, None, :]
    sine = jnp.sin(angle)[:, None, :]
    first = field[..., :half]
    second = field[..., half:]
    return jnp.concatenate(
        [first * cosine - second * sine, second * cosine + first * sine], axis=-1
    )


def shards(
    dims,
    tokens,
    positions,
    state,
    mix_gain,
    w_query,
    w_key,
    w_value,
    ret_gain,
    w_out,
    ffn_gain,
    routes,
    route_weights,
    expert_gate,
    expert_up,
    expert_down,
):
    seqs = tokens.shape[0]
    width = tokens.shape[1]
    heads = state.shape[1]
    head_k = state.shape[2]
    head_v = state.shape[3]
    normed_in = rms_scale(tokens, mix_gain)
    q_proj = jnp.dot(normed_in, w_query, preferred_element_type=jnp.float32).astype(jnp.bfloat16)
    k_proj = jnp.dot(normed_in, w_key, preferred_element_type=jnp.float32).astype(jnp.bfloat16)
    v_proj = jnp.dot(normed_in, w_value, preferred_element_type=jnp.float32).astype(jnp.bfloat16)
    queries = rotate(q_proj.astype(jnp.float32).reshape(seqs, heads, head_k), positions)
    key_rows = rotate(
        k_proj.astype(jnp.float32).reshape(seqs, heads, head_k), positions
    ) * head_k ** (-0.5)
    values = v_proj.astype(jnp.float32).reshape(seqs, heads, head_v)
    decays = 1.0 - jnp.exp2(-2.0 - jnp.arange(heads, dtype=jnp.float32))
    new_state = (
        decays[None, :, None, None] * state + key_rows[:, :, :, None] * values[:, :, None, :]
    )
    readout = jnp.einsum("thd,thdv->thv", queries, new_state, precision=lax.Precision.HIGHEST)
    centre = jnp.mean(readout, axis=-1, keepdims=True)
    variance = jnp.mean(jnp.square(readout - centre), axis=-1, keepdims=True)
    normed = ((readout - centre) * lax.rsqrt(variance + EPS)).reshape(
        seqs, heads * head_v
    ) * ret_gain
    mixed = normed.astype(jnp.bfloat16)
    attended = jnp.dot(
        mixed,
        gather_blocks(dims, w_out.T, 0).reshape(width, heads * head_v).T,
        preferred_element_type=jnp.float32,
    ).astype(jnp.bfloat16)
    resid = (tokens.astype(jnp.float32) + attended.astype(jnp.float32)).astype(jnp.bfloat16)
    normed_mid = rms_scale(resid, ffn_gain)
    count = lax.axis_size("ep")
    ids = jnp.arange(count, dtype=jnp.int32)
    wide_weights = jnp.sum(
        jnp.where(routes[:, :, None] == ids[None, None, :], route_weights[:, :, None], 0.0), axis=1
    )
    high = wide_weights.astype(jnp.bfloat16)
    low = (wide_weights - high.astype(jnp.float32)).astype(jnp.bfloat16)
    fill = -(-2 * count // 128) * 128 - 2 * count
    block = jnp.concatenate(
        [normed_mid, high, low, jnp.zeros((seqs, fill), jnp.bfloat16)], axis=1
    )
    block = jnp.pad(block, ((0, -(-seqs // PAD) * PAD - seqs), (0, 0)))
    result = experts(dims, block, resid, expert_gate, expert_up, expert_down, 1)
    return (result, new_state)


def solution(mesh):
    placed = (
        P("ep", None),
        P("ep"),
        P("ep", None, None, None),
        P(),
        P(),
        P(),
        P(),
        P(),
        P(None, "ep"),
        P(),
        P("ep", None),
        P("ep", None),
        P("ep", None, None),
        P("ep", None, None),
        P("ep", None, None),
    )
    return jax.shard_map(
        functools.partial(shards, layout_of(mesh)),
        mesh=mesh,
        in_specs=placed,
        out_specs=(P("ep", None), P("ep", None, None, None)),
        check_vma=False,
    )
```

time: 160 us -> 104 us (0.65)
  Pallas kernels: 0 us -> 77.6 us
  waiting for transfers between devices: 77.6 us -> 0 us
  blocking collectives: 29.4 us -> 0 us
  between operations: 14.3 us -> 0.92 us
  matrix products: 23.4 us -> 15.4 us
  starting transfers between devices: 3.66 us -> 0 us
    pallas_call x0 -> x2, Pallas kernels: none -> 77.6 us  [the longest x1 43.2 us: experts(): pl.pallas_call(functools.partial(experts_kernel, dims, seqs, width), out_...]
    all_gather x1 -> x0, waiting for transfers between devices: 50.9 us -> none  [shards(): lax.all_gather(w_out, 'ep', axis=1, tiled=True)]
    all_to_all x1 -> x0, blocking collectives: 29.4 us -> none  [shards(): lax.all_to_all(outgoing, 'ep', split_axis=0, concat_axis=0, tiled=True)]
    all_to_all x1 -> x0, waiting for transfers between devices: 26 us -> none  [shards(): lax.all_to_all(served, 'ep', split_axis=0, concat_axis=0, tiled=True)]
    dot_general x5 -> x1, matrix products: 11.6 us -> 3.51 us  [shards(): jnp.dot(mixed, gather_blocks(dims, w_out.T, 0).reshape(width, heads * hea...]
    all_to_all x1 -> x0, starting transfers between devices: 3.63 us -> none  [shards(): lax.all_to_all(served, 'ep', split_axis=0, concat_axis=0, tiled=True)]
    unnamed x28 -> x24, local copies, waits for them, and re-layouts: 1.38 us -> 4.76 us
    reshape x3 -> x0, local copies, waits for them, and re-layouts: 2.85 us -> none  [the longest x1 1.45 us: shards(): outgoing = outgoing.astype(jnp.bfloat16).reshape(experts, capacity, width)]
  transfers between devices with their start and end apart: 2 -> 0, of which waited for: 2 -> 0; matrix products, arithmetic and copies ran while one was open for 10% -> 0% of each run, Pallas kernels for 0% -> 0%
where the time goes in v1:
time: 104 us; the launch traced here: 103 us
  Pallas kernels  77.6 us (75%)
  matrix products  15.4 us (15%)
  local copies, waits for them, and re-layouts  5.69 us (5%)
  other arithmetic  3.71 us (4%)
    pallas_call x1, Pallas kernels, experts(): pl.pallas_call(functools.partial(experts_kernel, dims, seqs, width), out_...  43.2 us
    pallas_call x1, Pallas kernels, gather_blocks(): pl.pallas_call(functools.partial(gather_kernel, dims), out_shape=jax.Shap...  34.4 us
    unnamed x24, local copies, waits for them, and re-layouts  4.76 us
    dot_general x1, matrix products, shards(): jnp.einsum('thd,thdv->thv', queries, new_state, precision=lax.Precision.H...  4.59 us
    dot_general x1, matrix products, shards(): jnp.dot(mixed, gather_blocks(dims, w_out.T, 0).reshape(width, heads * hea...  3.51 us
    dot_general x1, matrix products, shards(): jnp.dot(normed_in, w_value, preferred_element_type=jnp.float32)  3.09 us
    dot_general x1, matrix products, shards(): jnp.dot(normed_in, w_query, preferred_element_type=jnp.float32)  2.1 us
    dot_general x1, matrix products, shards(): jnp.dot(normed_in, w_key, preferred_element_type=jnp.float32)  2.1 us

profile of v1, /device:TPU:0, one launch (start us, length us, event | category | flops | bytes accessed | tf_op | source)
XLA Modules:
  0.0 103.3 jit_solution(16395400575335965410)
XLA Ops:
  0.7 1.1 %fusion.9 = f32[20]{0:T(128)S(1)} fusion(bf16[20,2048]{1,0:T(8,128)(2,1)} %param.15), kind=kLoop, calls=%fused_computation.18 | loop fusion | flops 122860 | bytes 82000 | tf_op jit(solution)/shard_map/reduce_sum | solution.py:410
  1.7 2.1 %fusion.5 = f32[20,512]{1,0:T(8,128)S(1)} fusion(bf16[2048,512]{1,0:T(8,128)(2,1)} %param.19, bf16[20,2048]{1,0:T(8,128)(2,1)} %param.15, f32[2048]{0:T(1024)} %param.18, f32[20]{0:T(128)S(1)} %add_rsqrt_fusion.2), kind=kOutput, calls=%fused_computation.10 | convolution fusion | flops 42127360 | bytes 2228304 | tf_op jit(solution)/shard_map/dot_general | solution.py:451
  3.8 0.1 reshape.138
  3.9 2.1 %fusion.4 = f32[20,512]{1,0:T(8,128)S(1)} fusion(bf16[2048,512]{1,0:T(8,128)(2,1)} %param.20, bf16[20,2048]{1,0:T(8,128)(2,1)} %param.15, f32[2048]{0:T(1024)} %param.18, f32[20]{0:T(128)S(1)} %add_rsqrt_fusion.2), kind=kOutput, calls=%fused_computation.8 | convolution fusion | flops 42127360 | bytes 2228304 | tf_op jit(solution)/shard_map/dot_general | solution.py:452
  6.2 0.1 multiply_cosine_fusion
  6.3 0.1 multiply_subtract_fusion
  6.4 0.1 pad_maximum_fusion
  6.5 3.1 %fusion.3 = f32[20,1024]{1,0:T(8,128)S(1)} fusion(bf16[2048,1024]{1,0:T(8,128)(2,1)} %param.21, bf16[20,2048]{1,0:T(8,128)(2,1)S(1)} %copy-done.2, f32[2048]{0:T(1024)S(1)} %copy-done.4, f32[20]{0:T(128)S(1)} %add_rsqrt_fusion.2), kind=kOutput, calls=%fused_computation.6 | convolution fusion | flops 84090880 | bytes 4366416 | tf_op jit(solution)/shard_map/dot_general | solution.py:453
  9.7 0.2 copy-done.1
  9.9 1.7 %multiply_add_fusion = f32[20,8,64,128]{3,2,1,0:T(8,128)S(1)} fusion(f32[20,8,64,128]{3,2,1,0:T(8,128)S(1)} %copy-done.1, f32[20,8,128]{2,1,0:T(8,128)S(1)} %slice.20, f32[20,8,64]{2,1,0:T(8,128)S(1)} %get-tuple-element.15, f32[8]{0:T(128)S(1)} %exponential_subtract_fusion), kind=kLoop, calls=%fused_computation | loop fusion | flops 3932160 | bytes 10608672 | tf_op jit(solution)/shard_map/add | solution.py:461
  11.6 2.3 %copy-done = f32[20,8,64,128]{3,2,1,0:T(8,128)} copy-done((f32[20,8,64,128]{3,2,1,0:T(8,128)}, f32[20,8,64,128]{3,2,1,0:T(8,128)S(1)}, u32[]{:S(2)}) %copy-start) | copy-done | bytes 5242904
  13.9 4.6 %fusion.15 = f32[20,8,1,128]{3,2,1,0:T(1,128)S(1)} fusion(f32[20,8,64,1]{2,3,1,0:T(1,128)S(1)} %bitcast.27, f32[20,8,64,128]{3,2,1,0:T(8,128)S(1)} %multiply_add_fusion), kind=kOutput, calls=%fused_computation.40 | convolution fusion | flops 15728640 | bytes 5365760 | tf_op jit(solution)/shard_map/thd,thdv->thv/dot_general | solution.py:463
  18.5 0.1 reduce_sum.46
  18.6 0.2 multiply_reduce_fusion
  18.8 0.1 multiply_convert_fusion
  19.0 34.4 %gather_blocks.1 = bf16[32,64,1024]{2,1,0:T(8,128)(2,1)} custom-call(bf16[64,1024]{1,0:T(8,128)(2,1)} %bitcast.30), custom_call_target="tpu_custom_call" | custom-call | tf_op jit(solution)/shard_map/gather_blocks/pallas_call | solution.py:201
  53.4 3.5 %fusion.6 = (f32[20]{0:T(128)S(1)}, bf16[20,2048]{1,0:T(8,128)(2,1)S(1)}) fusion(bf16[20,1024]{1,0:T(8,128)(2,1)S(1)} %bitcast.28, bf16[2048,1024]{1,0:T(8,128)(2,1)} %bitcast.21, bf16[20,2048]{1,0:T(8,128)(2,1)} %param.15), kind=kOutput, calls=%fused_computation.15 | convolution fusion | flops 84213744 | bytes 4399184 | tf_op jit(solution)/shard_map/dot_general | solution.py:470
  56.9 0.6 copy-done.3
  57.6 0.1 fusion.8
  57.7 0.1 select_reduce_fusion
  57.8 0.1 concatenate.15
  57.9 0.6 pad.4.own
  58.6 43.2 %experts.1 = bf16[20,2048]{1,0:T(8,128)(2,1)} custom-call(bf16[24,2176]{1,0:T(8,128)(2,1)} %pad.4.own, bf16[20,2048]{1,0:T(8,128)(2,1)} %copy-done.3, bf16[1,2048,512]{2,1,0:T(8,128)(2,1)} %gate_hbm.1, bf16[1,2048,512]{2,1,0:T(8,128)(2,1)} %up_hbm.1, bf16[1,512,2048]{2,1,0:T(8,128)(2,1)} %down_hbm.1), custom_call_target="tpu_custom_call" | custom-call | tf_op jit(solution)/shard_map/experts/pallas_call | solution.py:386
  101.8 1.5 %copy.24 = bf16[20,2048]{1,0:T(8,128)(2,1)} copy(bf16[20,2048]{1,0:T(8,128)(2,1)} %experts.1) | data formatting | bytes 163840
  (31 shorter events, 0.3 us)
Async XLA Ops:
  0.6 5.9 %copy-start.2 = (bf16[20,2048]{1,0:T(8,128)(2,1)S(1)}, bf16[20,2048]{1,0:T(8,128)(2,1)}, u32[]{:S(2)}) copy-start(bf16[20,2048]{1,0:T(8,128)(2,1)} %param.15) | copy-start | bytes 245764
  0.6 5.9 %copy-start.4 = (f32[2048]{0:T(1024)S(1)}, f32[2048]{0:T(1024)}, u32[]{:S(2)}) copy-start(f32[2048]{0:T(1024)} %param.18) | copy-start | bytes 24580
  0.7 5.5 %copy-start.9 = (s32[20]{0:T(128)S(1)}, s32[20]{0:T(128)}, u32[]{:S(2)}) copy-start(s32[20]{0:T(128)} %param.16) | copy-start | bytes 244
  6.1 3.8 %copy-start.1 = (f32[20,8,64,128]{3,2,1,0:T(8,128)S(1)}, f32[20,8,64,128]{3,2,1,0:T(8,128)}, u32[]{:S(2)}) copy-start(f32[20,8,64,128]{3,2,1,0:T(8,128)} %param.17) | copy-start | bytes 15728644
  11.6 2.4 %copy-start = (f32[20,8,64,128]{3,2,1,0:T(8,128)}, f32[20,8,64,128]{3,2,1,0:T(8,128)S(1)}, u32[]{:S(2)}) copy-start(f32[20,8,64,128]{3,2,1,0:T(8,128)S(1)} %multiply_add_fusion) | copy-start | bytes 15728644
  11.6 7.2 %copy-start.6 = (f32[1024]{0:T(1024)S(1)}, f32[1024]{0:T(1024)}, u32[]{:S(2)}) copy-start(f32[1024]{0:T(1024)} %param.22) | copy-start | bytes 12292
  19.0 38.6 %copy-start.5 = (f32[2048]{0:T(1024)S(1)}, f32[2048]{0:T(1024)}, u32[]{:S(2)}) copy-start(f32[2048]{0:T(1024)} %param.24) | copy-start | bytes 24580
  19.0 38.7 %copy-start.7 = (f32[20,6]{0,1:T(8,128)S(1)}, f32[20,6]{0,1:T(8,128)}, u32[]{:S(2)}) copy-start(f32[20,6]{0,1:T(8,128)} %param.26) | copy-start | bytes 1444
  19.0 38.7 %copy-start.8 = (s32[20,6]{0,1:T(8,128)S(1)}, s32[20,6]{0,1:T(8,128)}, u32[]{:S(2)}) copy-start(s32[20,6]{0,1:T(8,128)} %param.25) | copy-start | bytes 1444
  56.9 0.7 copy-start.3

commit v2 on v1

--- a/solution.py
+++ b/solution.py
@@ -48,14 +48,30 @@
     def at(self, dz, dy, dx, dc=0):
         total = 0
         for size, here, move in zip(self.dims, self.spot, (dz, dy, dx, dc)):
-            total = total * size + (here + move) % size if move % size else total * size + here
+            total = total * size + self.moved(size, here, move)
         return total
 
-    def greet(self):
+    @staticmethod
+    def moved(size, here, move):
+        if not move % size:
+            return here
+        if size & (size - 1):
+            return (here + move) % size
+        bit = 1
+        there = here
+        while bit < size:
+            if abs(move) & bit:
+                there = there + bit - 2 * bit * ((here // bit) % 2)
+            bit *= 2
+        return there
+
+    def greet(self, corners=False):
         depth, rows, cols, cores = self.dims
         moves = [(d, 0, 0, 0) for d in range(1, depth)]
         moves += [(0, d, 0, 0) for d in range(1, rows)]
         moves += [(0, 0, d, 0) for d in range(1, cols)]
+        if corners:
+            moves += [(0, dy, dx, 0) for dy in range(1, rows) for dx in range(1, cols)]
         moves += [(0, 0, 0, d) for d in range(1, cores)]
         barrier = pltpu.get_barrier_semaphore()
         for move in moves:
@@ -175,35 +191,195 @@
     return view
 
 
-def gather_kernel(dims, own, out, load, send, recv):
+def retain_kernel(
+    dims, sizes, own, normed, wq_hbm, wk_hbm, wv_hbm, cosine, sine, gain, state_hbm,
+    out, key_out, value_out,
+    wq, wk, wv, state, flip, qcols, kcols, values, decay, readout, lines, mixed, attended, back,
+    load, wload, sload, send, recv,
+):
+    heads, head_k, head_v = sizes
     place = Place(dims)
-    fill = pltpu.make_async_copy(own, out.at[place.me], load)
+    seqs = normed.shape[0]
+    depth, rows, cols, cores = dims
+    names = retain_names(dims)
+
+    def slot(dz, dc):
+        return place.moved(depth, place.spot[0], dz) * cores + place.moved(cores, place.spot[3], dc)
+
+    def remote(name, src, dst, target):
+        m = names[name]
+        return pltpu.make_async_remote_copy(
+            src_ref=src, dst_ref=dst, send_sem=send.at[m], recv_sem=recv.at[m],
+            device_id=(place.at(*target),), device_id_type=MESH,
+        )
+
+    fill = pltpu.make_async_copy(own, lines.at[slot(0, 0)], load)
     fill.start()
-    place.greet()
+    weights = [
+        pltpu.make_async_copy(src, dst, wload.at[i])
+        for i, (src, dst) in enumerate([(wq_hbm, wq), (wk_hbm, wk), (wv_hbm, wv)])
+    ]
+    for copy in weights:
+        copy.start()
+    taken = pltpu.make_async_copy(state_hbm, state, sload)
+    taken.start()
+    place.greet(corners=True)
     fill.wait()
-    g = Gather(place, halves(out, out.shape[2]), send, recv)
-    depth = dims[0]
-    for t in range(depth + 3):
-        if t < depth:
-            g.first(t)
-        if 0 <= t - 1 < depth:
-            g.second(t - 1)
-        if 0 <= t - 2 < depth:
-            g.third(t - 2)
-        if 0 <= t - 3 < depth:
-            g.fourth(t - 3)
-    g.finish()
-
-
-def gather_blocks(dims, block, collective):
-    count = math.prod(dims)
-    messages = len(gather_names(dims))
+    sent = []
+
+    def put(*args):
+        copy = remote(*args)
+        copy.start()
+        sent.append(copy)
+
+    for dz in range(1, depth):
+        put(("z", dz), lines.at[slot(0, 0)], lines.at[slot(0, 0)], (-dz, 0, 0, 0))
+    for dc in range(1, cores):
+        put(("c", 0, dc), lines.at[slot(0, 0)], lines.at[slot(0, 0)], (0, 0, 0, -dc))
+
+    def rotated(field):
+        lane = lax.broadcasted_iota(jnp.int32, field.shape, 1) % head_k
+        total = field.shape[1]
+        ahead = pltpu.roll(field, total - head_k // 2, 1)
+        behind = pltpu.roll(field, head_k // 2, 1)
+        return field * cosine[...] + jnp.where(lane < head_k // 2, -ahead, behind) * sine[...]
+
+    def columns(field, target):
+        flip[...] = jnp.zeros_like(flip)
+        flip[pl.ds(0, seqs), :] = field
+        target[...] = flip[...].T
+
+    def project(weight):
+        part = jnp.dot(normed[...], weight[...], preferred_element_type=jnp.float32)
+        return part.astype(jnp.bfloat16).astype(jnp.float32)
+
+    def queries():
+        weights[0].wait()
+        columns(rotated(project(wq)), qcols)
+
+    def keys():
+        weights[1].wait()
+        key_out[...] = rotated(project(wk)) * head_k ** (-0.5)
+        columns(key_out[...], kcols)
+
+    def others():
+        weights[2].wait()
+        part = project(wv)
+        value_out[...] = part
+        for h in range(heads):
+            values[:, h, :] = part[:, h * head_v : (h + 1) * head_v]
+            decay[pl.ds(h * head_k, head_k), :] = jnp.full((head_k, head_v), 1.0 - 2.0 ** (-2.0 - h), jnp.float32)
+        taken.wait()
+
+    def span(start, stop):
+        def one(t, carry):
+            lane = lax.broadcasted_iota(jnp.int32, qcols.shape, 1)
+            query = jnp.sum(jnp.where(lane == t, qcols[...], 0.0), axis=1, keepdims=True)
+            key = jnp.sum(jnp.where(lane == t, kcols[...], 0.0), axis=1, keepdims=True)
+            value = values[t]
+            outer = key.reshape(heads, head_k, 1) * value.reshape(heads, 1, head_v)
+            fresh = decay[...] * state[t] + outer.reshape(heads * head_k, head_v)
+            readout[t] = jnp.sum((query * fresh).reshape(heads, head_k, head_v), axis=1)
+            return carry
+
+        lax.fori_loop(start, stop, one, 0)
+
+    def close():
+        for h in range(heads):
+            read = readout[:, h, :]
+            apart = read - jnp.mean(read, axis=1, keepdims=True)
+            variance = jnp.mean(apart * apart, axis=1, keepdims=True)
+            lanes = pl.ds(h * head_v, head_v)
+            mixed[0, pl.ds(0, seqs), lanes] = (apart * lax.rsqrt(variance + EPS) * gain[:, lanes]).astype(mixed.dtype)
+
+    queries()
+    keys()
+    others()
+    span(0, seqs)
+    mixed[0] = jnp.zeros(mixed.shape[1:], mixed.dtype)
+    close()
+    moves = [(dy, dx) for dy in range(rows) for dx in range(cols)]
+    for i, (dy, dx) in enumerate(moves):
+        if i:
+            put(("m", dy, dx), mixed.at[0], mixed.at[i], (0, -dy, -dx, 0))
+    for dz in range(1, depth):
+        held = lines.at[slot(dz, 0)]
+        remote(("z", dz), held, held, (-dz, 0, 0, 0)).wait_recv()
+        for dc in range(1, cores):
+            put(("c", dz, dc), held, held, (0, 0, 0, -dc))
+    for i, (dy, dx) in enumerate(moves):
+        if i:
+            remote(("m", dy, dx), mixed.at[0], mixed.at[i], (0, -dy, -dx, 0)).wait_recv()
+    for dz in range(depth):
+        for dc in range(1, cores):
+            held = lines.at[slot(dz, dc)]
+            remote(("c", dz, dc), held, held, (0, 0, 0, -dc)).wait_recv()
+    tall = mixed.shape[1]
+    product = lax.dot_general(
+        mixed[...].reshape(len(moves) * tall, mixed.shape[2]),
+        lines[...].reshape(-1, lines.shape[2]),
+        (((1,), (1,)), ((), ())),
+        preferred_element_type=jnp.float32,
+    )
+    attended[...] = product.astype(attended.dtype).reshape(attended.shape)
+    for i, (dy, dx) in enumerate(moves):
+        if i:
+            put(("r", dy, dx), attended.at[i], back.at[i], (0, dy, dx, 0))
+    for i, (dy, dx) in enumerate(moves):
+        origin = place.moved(rows, place.spot[1], -dy) * cols + place.moved(cols, place.spot[2], -dx)
+        if i:
+            remote(("r", dy, dx), attended.at[i], back.at[i], (0, dy, dx, 0)).wait_recv()
+        out[origin] = back[i] if i else attended[0]
+    for copy in sent:
+        copy.wait_send()
+
+
+def retain_names(dims):
+    depth, rows, cols, cores = dims
+    names = [("z", dz) for dz in range(1, depth)]
+    names += [("c", dz, dc) for dz in range(depth) for dc in range(1, cores)]
+    names += [(k, dy, dx) for k in "mr" for dy in range(rows) for dx in range(cols) if dy or dx]
+    return {name: i for i, name in enumerate(names)}
+
+
+def retain(dims, sizes, block, normed, wq, wk, wv, cosine, sine, gain, state, collective):
+    heads, head_k, head_v = sizes
+    depth, rows, cols, cores = dims
+    messages = len(retain_names(dims))
+    seqs = normed.shape[0]
+    flat = (seqs, heads * head_k, head_v)
+    anywhere = pl.BlockSpec(memory_space=pl.ANY)
+    here = pl.BlockSpec(memory_space=pltpu.VMEM)
+    across = -(-seqs // 128) * 128
+    tall = -(-seqs // PAD) * PAD
+    some = depth * cores * block.shape[0]
+    plane = rows * cols
     return pl.pallas_call(
-        functools.partial(gather_kernel, dims),
-        out_shape=jax.ShapeDtypeStruct((count,) + block.shape, block.dtype),
-        in_specs=[pl.BlockSpec(memory_space=pl.ANY)],
-        out_specs=pl.BlockSpec(memory_space=pltpu.VMEM),
+        functools.partial(retain_kernel, dims, sizes),
+        out_shape=(
+            jax.ShapeDtypeStruct((plane, tall, some), jnp.bfloat16),
+            jax.ShapeDtypeStruct((seqs, heads * head_k), jnp.float32),
+            jax.ShapeDtypeStruct((seqs, heads * head_v), jnp.float32),
+        ),
+        in_specs=[anywhere, here, anywhere, anywhere, anywhere, here, here, here, anywhere],
+        out_specs=(here, here, here),
         scratch_shapes=[
+            pltpu.VMEM(wq.shape, wq.dtype),
+            pltpu.VMEM(wk.shape, wk.dtype),
+            pltpu.VMEM(wv.shape, wv.dtype),
+            pltpu.VMEM(flat, jnp.float32),
+            pltpu.VMEM((across, heads * head_k), jnp.float32),
+            pltpu.VMEM((heads * head_k, across), jnp.float32),
+            pltpu.VMEM((heads * head_k, across), jnp.float32),
+            pltpu.VMEM((seqs, heads, head_v), jnp.float32),
+            pltpu.VMEM((heads * head_k, head_v), jnp.float32),
+            pltpu.VMEM((seqs, heads, head_v), jnp.float32),
+            pltpu.VMEM((depth * cores,) + block.shape, block.dtype),
+            pltpu.VMEM((plane, tall, heads * head_v), jnp.bfloat16),
+            pltpu.VMEM((plane, tall, some), jnp.bfloat16),
+            pltpu.VMEM((plane, tall, some), jnp.bfloat16),
+            pltpu.SemaphoreType.DMA,
+            pltpu.SemaphoreType.DMA((3,)),
             pltpu.SemaphoreType.DMA,
             pltpu.SemaphoreType.DMA((messages,)),
             pltpu.SemaphoreType.DMA((messages,)),
@@ -211,8 +387,8 @@
         compiler_params=pltpu.CompilerParams(
             collective_id=collective, has_side_effects=True, vmem_limit_bytes=VMEM_LIMIT
         ),
-        name="gather_blocks",
-    )(block)
+        name="retain",
+    )(block, normed, wq, wk, wv, cosine, sine, gain, state.reshape(flat))
 
 
 class Reduce:
@@ -332,7 +508,7 @@
         step -= 1
 
     def serve(dz):
-        base = ((place.spot[0] + dz) % depth) * plane
+        base = place.moved(depth, place.spot[0], dz) * plane
         extra = held.shape[2] - width
         lane = lax.broadcasted_iota(jnp.int32, (step * padded, extra), 1)
         pick = jnp.logical_or(lane == place.me, lane == place.me + count)
@@ -411,17 +587,8 @@
     return (scaled * gain).astype(jnp.bfloat16)
 
 
-def rotate(field, spots):
-    half = field.shape[-1] // 2
-    freqs = jnp.exp(-math.log(10000.0) * jnp.arange(half, dtype=jnp.float32) / half)
-    angle = spots.astype(jnp.float32)[:, None] * freqs[None, :]
-    cosine = jnp.cos(angle)[:, None, :]
-    sine = jnp.sin(angle)[:, None, :]
-    first = field[..., :half]
-    second = field[..., half:]
-    return jnp.concatenate(
-        [first * cosine - second * sine, second * cosine + first * sine], axis=-1
-    )
+def padded_rows(rows):
+    return jnp.pad(rows, ((0, -(-rows.shape[0] // PAD) * PAD - rows.shape[0]), (0, 0)))
 
 
 def shards(
@@ -448,33 +615,24 @@
     head_k = state.shape[2]
     head_v = state.shape[3]
     normed_in = rms_scale(tokens, mix_gain)
-    q_proj = jnp.dot(normed_in, w_query, preferred_element_type=jnp.float32).astype(jnp.bfloat16)
-    k_proj = jnp.dot(normed_in, w_key, preferred_element_type=jnp.float32).astype(jnp.bfloat16)
-    v_proj = jnp.dot(normed_in, w_value, preferred_element_type=jnp.float32).astype(jnp.bfloat16)
-    queries = rotate(q_proj.astype(jnp.float32).reshape(seqs, heads, head_k), positions)
-    key_rows = rotate(
-        k_proj.astype(jnp.float32).reshape(seqs, heads, head_k), positions
-    ) * head_k ** (-0.5)
-    values = v_proj.astype(jnp.float32).reshape(seqs, heads, head_v)
+    half = head_k // 2
+    freqs = jnp.exp(-math.log(10000.0) * jnp.arange(half, dtype=jnp.float32) / half)
+    angle = positions.astype(jnp.float32)[:, None] * jnp.tile(freqs, 2 * heads)[None, :]
+    columns, key_rows, values = retain(
+        dims, (heads, head_k, head_v), w_out.T, normed_in, w_query, w_key, w_value,
+        jnp.cos(angle), jnp.sin(angle), ret_gain.reshape(1, -1), state, 0,
+    )
+    key_rows = key_rows.reshape(seqs, heads, head_k)
+    values = values.reshape(seqs, heads, head_v)
     decays = 1.0 - jnp.exp2(-2.0 - jnp.arange(heads, dtype=jnp.float32))
     new_state = (
         decays[None, :, None, None] * state + key_rows[:, :, :, None] * values[:, :, None, :]
     )
-    readout = jnp.einsum("thd,thdv->thv", queries, new_state, precision=lax.Precision.HIGHEST)
-    centre = jnp.mean(readout, axis=-1, keepdims=True)
-    variance = jnp.mean(jnp.square(readout - centre), axis=-1, keepdims=True)
-    normed = ((readout - centre) * lax.rsqrt(variance + EPS)).reshape(
-        seqs, heads * head_v
-    ) * ret_gain
-    mixed = normed.astype(jnp.bfloat16)
-    attended = jnp.dot(
-        mixed,
-        gather_blocks(dims, w_out.T, 0).reshape(width, heads * head_v).T,
-        preferred_element_type=jnp.float32,
-    ).astype(jnp.bfloat16)
+    count = lax.axis_size("ep")
+    columns = columns[:, :seqs].reshape(dims[1] * dims[2], seqs, dims[0], -1)
+    attended = jnp.transpose(columns, (1, 2, 0, 3)).reshape(seqs, width)
     resid = (tokens.astype(jnp.float32) + attended.astype(jnp.float32)).astype(jnp.bfloat16)
     normed_mid = rms_scale(resid, ffn_gain)
-    count = lax.axis_size("ep")
     ids = jnp.arange(count, dtype=jnp.int32)
     wide_weights = jnp.sum(
         jnp.where(routes[:, :, None] == ids[None, None, :], route_weights[:, :, None], 0.0), axis=1
@@ -485,7 +643,7 @@
     block = jnp.concatenate(
         [normed_mid, high, low, jnp.zeros((seqs, fill), jnp.bfloat16)], axis=1
     )
-    block = jnp.pad(block, ((0, -(-seqs // PAD) * PAD - seqs), (0, 0)))
+    block = padded_rows(block)
     result = experts(dims, block, resid, expert_gate, expert_up, expert_down, 1)
     return (result, new_state)
 

time: 104 us -> 89.2 us (0.86)
  matrix products: 15.4 us -> 0 us
  other arithmetic: 3.71 us -> 13.5 us
  Pallas kernels: 77.6 us -> 69.8 us
    dot_general x5 -> x0, matrix products: 15.4 us -> none  [the longest x1 4.59 us: shards(): jnp.einsum('thd,thdv->thv', queries, new_state, precision=lax.Precision.H...]
    pallas_call x1, Pallas kernels: 34.4 us -> 24.6 us  [retain(): pl.pallas_call(functools.partial(retain_kernel, dims, sizes), out_shape=(...]
    add x1, other arithmetic: 1.68 us -> 6.39 us  [shards(): decays[None, :, None, None] * state]
    unnamed x24 -> x8, local copies, waits for them, and re-layouts: 4.76 us -> 2.19 us
    pallas_call x1, Pallas kernels: 43.2 us -> 45.3 us  [experts(): pl.pallas_call(functools.partial(experts_kernel, dims, seqs, width), out_...]
    convert_element_type x1 -> x2, other arithmetic: 0.09 us -> 1.71 us  [rms_scale(): return (scaled * gain).astype(jnp.bfloat16)]
    mul x1 -> x2, local copies, waits for them, and re-layouts: 0.01 us -> 1.52 us  [shards(): key_rows[:, :, :, None] * values[:, :, None, :]]
    convert_element_type x2, other arithmetic: 0.11 us -> 1.56 us  [the longest x1 0.91 us: shards(): attended.astype(jnp.float32)]
where the time goes in v2:
time: 89.2 us; the launch traced here: 88.8 us
  Pallas kernels  69.8 us (78%)
  other arithmetic  13.5 us (15%)
  local copies, waits for them, and re-layouts  4.73 us (5%)
    pallas_call x1, Pallas kernels, experts(): pl.pallas_call(functools.partial(experts_kernel, dims, seqs, width), out_...  45.3 us
    pallas_call x1, Pallas kernels, retain(): pl.pallas_call(functools.partial(retain_kernel, dims, sizes), out_shape=(...  24.6 us
    add x1, other arithmetic, shards(): decays[None, :, None, None] * state  6.39 us
    unnamed x8, local copies, waits for them, and re-layouts  2.19 us
    reduce_sum x2, other arithmetic, rms_scale(): jnp.mean(wide * wide, axis=-1, keepdims=True) + EPS  2.06 us

profile of v2, /device:TPU:0, one launch (start us, length us, event | category | flops | bytes accessed | tf_op | source)
XLA Modules:
  0.0 88.8 jit_solution(9876132132345172742)
XLA Ops:
  0.6 0.7 convert_element_type.44
  1.3 1.0 %fusion.3 = f32[20]{0:T(128)S(1)} fusion(bf16[20,2048]{1,0:T(8,128)(2,1)} %param.15), kind=kLoop, calls=%fused_computation.9 | loop fusion | flops 122860 | bytes 82000 | tf_op jit(solution)/shard_map/reduce_sum | solution.py:586
  2.4 0.1 mul.87
  2.4 0.8 select_reduce_fusion
  3.3 0.9 %multiply_sine_fusion = (f32[20,512]{1,0:T(8,128)}, f32[20,512]{1,0:T(8,128)}) fusion(f32[512]{0:T(512)S(1)} %mul.87, f32[20]{0:T(128)S(1)} %convert_element_type.44), kind=kLoop, calls=%fused_computation.16 | loop fusion | flops 10240 | bytes 84048 | tf_op jit(solution)/shard_map/sin | solution.py:623
  4.2 1.6 %fusion.5.normed = bf16[20,2048]{1,0:T(8,128)(2,1)} fusion(bf16[20,2048]{1,0:T(8,128)(2,1)} %param.15, f32[2048]{0:T(1024)} %param.18, f32[20]{0:T(128)S(1)} %add_rsqrt_fusion.1), kind=kLoop, calls=%fused_computation.11 | loop fusion | flops 163840 | bytes 172112 | tf_op jit(solution)/shard_map/convert_element_type | solution.py:587
  5.8 24.6 %retain.1 = (bf16[4,24,512]{2,1,0:T(8,128)(2,1)}, f32[20,512]{1,0:T(8,128)}, f32[20,1024]{1,0:T(8,128)}) custom-call(bf16[64,1024]{1,0:T(8,128)(2,1)} %bitcast.11, bf16[20,2048]{1,0:T(8,128)(2,1)} %fusion.5.normed, bf16[2048,512]{1,0:T(8,128)(2,1)} %wq_hbm.1, bf16[2048,512]{1,0:T(8,128)(2,1)} %wk_hbm.1, bf16[2048,1024]{1,0:T(8,128)(2,1)} %wv_hbm.1, ...), custom_call_target="tpu_custom_call" | custom-call | tf_op jit(solution)/shard_map/retain/pallas_call | solution.py:357
  30.4 1.5 %mul.97 = f32[20,8,64]{2,1,0:T(8,128)} reshape(f32[20,512]{1,0:T(8,128)} %get-tuple-element.6) | data formatting | bytes 81920 | tf_op jit(solution)/shard_map/mul | solution.py:629
  31.9 0.9 %slice_convert_fusion = f32[4,20,512]{2,1,0:T(8,128)S(1)} fusion(bf16[4,24,512]{2,1,0:T(8,128)(2,1)} %get-tuple-element.5), kind=kLoop, calls=%fused_computation.13 | loop fusion | flops 40960 | bytes 245760 | tf_op jit(solution)/shard_map/convert_element_type | solution.py:634
  32.8 0.1 reshape.56
  32.9 0.1 copy.25
  32.9 0.1 reshape.54
  33.0 1.0 %fusion = (f32[20]{0:T(128)S(1)}, bf16[20,2048]{1,0:T(8,128)(2,1)S(1)}) fusion(f32[20,2048]{1,0:T(8,128)S(1)} %reshape.54, bf16[20,2048]{1,0:T(8,128)(2,1)} %param.15), kind=kLoop, calls=%fused_computation.6 | loop fusion | flops 245740 | bytes 327760 | tf_op jit(solution)/shard_map/reduce_sum | solution.py:586
  34.1 0.6 copy-done
  34.7 0.0 copy-done.2
  34.7 0.1 fusion.2
  34.8 0.1 concatenate.3
  34.9 0.7 pad.4.own
  35.5 45.3 %experts.1 = bf16[20,2048]{1,0:T(8,128)(2,1)} custom-call(bf16[24,2176]{1,0:T(8,128)(2,1)} %pad.4.own, bf16[20,2048]{1,0:T(8,128)(2,1)} %copy-done, bf16[1,2048,512]{2,1,0:T(8,128)(2,1)} %gate_hbm.1, bf16[1,2048,512]{2,1,0:T(8,128)(2,1)} %up_hbm.1, bf16[1,512,2048]{2,1,0:T(8,128)(2,1)} %down_hbm.1), custom_call_target="tpu_custom_call" | custom-call | tf_op jit(solution)/shard_map/experts/pallas_call | solution.py:562
  80.8 0.9 %copy.28 = f32[3,8,8,128]{3,2,1,0:T(8,128)S(1)} copy(f32[3,8,8,128]{3,1,2,0:T(8,128)} %bitcast.12) | data formatting | bytes 196608
  81.7 0.0 copy-start.1
  81.8 6.4 %multiply_add_fusion = f32[20,8,64,128]{3,2,1,0:T(8,128)} fusion(f32[20,8,64,128]{3,2,1,0:T(8,128)} %param.17, f32[20,8,128]{2,1,0:T(8,128)S(1)} %slice.4, f32[20,8,64]{2,1,0:T(8,128)} %mul.97, f32[8]{0:T(128)S(1)} %exponential_subtract_fusion), kind=kLoop, calls=%fused_computation | loop fusion | flops 3932160 | bytes 10608672 | tf_op jit(solution)/shard_map/add | solution.py:629
  88.2 0.0 copy-done.1
  88.2 0.6 copy.30
  (10 shorter events, 0.1 us)
Async XLA Ops:
  5.8 28.9 %copy-start.2 = (f32[2048]{0:T(1024)S(1)}, f32[2048]{0:T(1024)}, u32[]{:S(2)}) copy-start(f32[2048]{0:T(1024)} %param.24) | copy-start | bytes 24580
  34.0 0.6 copy-start
  81.7 6.4 %copy-start.1 = (bf16[20,2048]{1,0:T(8,128)(2,1)S(1)}, bf16[20,2048]{1,0:T(8,128)(2,1)}, u32[]{:S(2)}) copy-start(bf16[20,2048]{1,0:T(8,128)(2,1)} %experts.1) | copy-start | bytes 245764
